TPU v7x, 256 devices: a whole 4x4x8 slice. The times are simulated.
256 devices in a mesh: ep: 16 (over y, x), tp: 16 (over z, core).
Axes of the slice: x: 4, y: 4, z: 8, core: 2. Of those that a mesh axis runs over, the one named last changes fastest.
Arguments:
- tokens: bfloat16 [8192, 1024], P(('ep', 'tp')), may hold values from -6 to 6
- norm_gain: float32 [1024], replicated, may hold values from 0.5 to 1.5
- routing: int32 [8192, 2], P('ep'), may hold values from 0 to 31, as said below
- gate_share: float32 [8192, 2], P('ep'), may hold values from 0.5 to 1.5
- w_gate: bfloat16 [32, 1024, 256], P('ep', None, 'tp'), may hold values from -0.1875 to 0.1875
- w_up: bfloat16 [32, 1024, 256], P('ep', None, 'tp'), may hold values from -0.1875 to 0.1875
- w_down: bfloat16 [32, 256, 1024], P('ep', 'tp'), may hold values from -0.375 to 0.375
Outputs:
- mixed_out: bfloat16 [8192, 1024], P('ep', 'tp')
Inputs may be any that keep to these rules, and one draw needn't show every extreme that they name: `routing`: each row names two different experts whose ids lie in the same block of 8 consecutive ids. In each aligned block of 512 rows (the tokens of one index of ep) no expert is named by more than 64 rows, and some expert is named by exactly 64.
All inputs are finite; a program needn't handle non-finite values.
Results may differ from a plain program's by a relative error of at most 0.0015.
Values may be sent and summed in bfloat16 or wider, within the bound.
No kernel may reach another device: no remote copies, remote signals or barrier semaphores. Data moves between devices by JAX's collectives and lax.ppermute only.
A program may use at most 64 MiB of HBM per device.

v0:
```python
import jax
import jax.numpy as jnp
from jax import lax
from jax.sharding import PartitionSpec as P

epsilon = 1e-06


def in_order(parts, dim):
    shape = list(parts.shape[1:])
    shape[dim] *= parts.shape[0]
    return jnp.moveaxis(parts, 0, dim).reshape(shape)


def gather_together(arrays, axis, dims):
    flat = jnp.concatenate([a.reshape(-1) for a in arrays])
    lines, at, outs = (lax.all_gather(flat, axis), 0, [])
    for a, dim in zip(arrays, dims):
        parts = lines[:, at : at + a.size].reshape(-1, *a.shape)
        outs.append(in_order(parts, dim))
        at += a.size
    return tuple(outs)


def norm_rows(tokens, norm_gain):
    as_float = tokens.astype(jnp.float32)
    scaled = as_float * lax.rsqrt(jnp.mean(as_float * as_float, axis=-1, keepdims=True) + epsilon)
    return (scaled * norm_gain.astype(jnp.float32)).astype(jnp.bfloat16)


def fill_buffer(group, flat_target, slots, model_width):
    buffer = jnp.zeros((slots, model_width), jnp.bfloat16)
    return buffer.at[flat_target].set(jnp.repeat(group, 2, axis=0))


def body(tokens, norm_gain, routing, gate_share, w_gate, w_up, w_down):
    ep_size = lax.axis_size("ep")
    tp_size = lax.axis_size("tp")
    local_experts = w_gate.shape[0]
    experts = local_experts * ep_size
    group_rows = routing.shape[0]
    capacity = group_rows * 4 // experts
    model_width = tokens.shape[1]
    columns = model_width // tp_size
    normed = norm_rows(tokens, norm_gain)
    onehot = (routing[:, :, None] == jnp.arange(experts, dtype=jnp.int32)[None, None, :]).astype(
        jnp.int32
    )
    flat_hot = onehot.reshape(group_rows * 2, experts)
    ranking = jnp.cumsum(flat_hot, axis=0) - 1
    slot_pos = jnp.sum(ranking * flat_hot, axis=1).reshape(group_rows, 2)
    target = (routing * capacity + slot_pos).astype(jnp.int32)
    flat_target = target.reshape(-1)
    slice_len = capacity // tp_size
    tp_index = lax.axis_index("tp")
    group = lax.all_gather(normed, "tp", axis=0, tiled=True)
    buffer = fill_buffer(group, flat_target, experts * capacity, model_width)
    shaped = buffer.reshape(ep_size, local_experts, capacity, model_width)
    mine = lax.dynamic_slice_in_dim(shaped, tp_index * slice_len, slice_len, 2)
    mine = mine.reshape(ep_size, local_experts * slice_len, model_width)
    landed = lax.all_to_all(mine, "ep", split_axis=0, concat_axis=0, tiled=True)
    landed = landed.reshape(ep_size, local_experts, slice_len, model_width).transpose(1, 0, 2, 3)
    landed = landed.reshape(local_experts, ep_size * slice_len, model_width)
    full_gate, full_up, full_down = gather_together((w_gate, w_up, w_down), "tp", (2, 2, 1))
    gate_sum = jnp.einsum("erd,edh->erh", landed, full_gate, preferred_element_type=jnp.float32)
    up_sum = jnp.einsum("erd,edh->erh", landed, full_up, preferred_element_type=jnp.float32)
    hidden = (jax.nn.silu(gate_sum) * up_sum).astype(jnp.bfloat16)
    produced = jnp.einsum(
        "erh,ehd->erd", hidden, full_down, preferred_element_type=jnp.float32
    ).astype(jnp.bfloat16)
    produced = produced.reshape(local_experts, ep_size, slice_len, model_width)
    blocks = lax.all_to_all(produced, "tp", split_axis=3, concat_axis=2, tiled=True)
    leaving = blocks.transpose(1, 0, 2, 3).reshape(ep_size, local_experts * capacity, columns)
    returned = lax.all_to_all(leaving, "ep", split_axis=0, concat_axis=0, tiled=True).reshape(
        experts * capacity, columns
    )
    picked_out = returned[target]
    mixed_out = jnp.sum(gate_share[:, :, None] * picked_out.astype(jnp.float32), axis=1)
    return mixed_out.astype(jnp.bfloat16)


def solution(mesh):
    return jax.shard_map(
        body,
        mesh=mesh,
        in_specs=(
            P(("ep", "tp"), None),
            P(),
            P("ep", None),
            P("ep", None),
            P("ep", None, "tp"),
            P("ep", None, "tp"),
            P("ep", "tp", None),
        ),
        out_specs=P("ep", "tp"),
        check_vma=False,
    )
```

profile of v0, /device:TPU:1, one launch (start us, length us, event | category | flops | bytes accessed | tf_op | source)
XLA Modules:
  0.0 184.5 jit_solution(3607458096180063243)
XLA Ops:
  6.5 1.0 fusion.4
  7.5 1.6 fusion.6
  9.2 1.1 copy.96
  10.3 0.3 reshape.123
  10.6 1.1 copy.97
  11.7 0.3 reshape.124
  12.1 0.9 copy.115
  12.9 0.7 pad_maximum_fusion
  13.7 0.1 copy.86
  13.8 0.2 eq.30
  14.0 0.2 eq.26
  14.2 9.0 %reduce-window.6 = s32[32,8,128]{2,1,0:T(8,128)S(1)} reduce-window(s32[32,8,128]{2,1,0:T(8,128)S(1)} %fusion.14, s32[]{:T(128)} %constant.13.clone.1), window={size=1x1x128 pad=0_0x0_0x127_0}, to_apply=%region_0.0 | reduce-window | flops 4161536 | bytes 262148 | tf_op jit(solution)/shard_map/reduce-window
  23.7 0.2 reshape.116
  24.0 0.2 copy.91
  24.2 0.2 reshape.117
  24.4 27.6 %all-gather.4.cloned.1.call-done = bf16[512,1024]{1,0:T(8,128)(2,1)} async-done(((bf16[32,1024]{1,0:T(8,128)(2,1)}), bf16[512,1024]{1,0:T(8,128)(2,1)}) %all-gather.4.cloned.1.call-update) | async-done | bytes 1048592 | tf_op jit(solution)/shard_map/all_gather | solution.py:56
  52.0 2.3 %broadcast_in_dim.7 = bf16[512,2,1024]{2,1,0:T(2,128)(2,1)S(1)} broadcast(bf16[512,1024]{1,0:T(8,128)(2,1)} %all-gather.4.cloned.1.call-done), dimensions={0,2} | broadcast | bytes 3145728 | tf_op jit(solution)/shard_map/broadcast_in_dim | solution.py:33
  54.3 2.3 %reshape.147 = bf16[1024,1024]{1,0:T(8,128)(2,1)} reshape(bf16[512,2,1024]{2,1,0:T(2,128)(2,1)S(1)} %broadcast_in_dim.7) | data formatting | bytes 4194304 | tf_op jit(solution)/shard_map/reshape | solution.py:33
  56.6 8.6 %scatter_custom_fusion = bf16[2048,1024]{1,0:T(8,128)(2,1)} fusion(s32[1024]{0:T(1024)S(1)} %bitcast.70, bf16[1024,1024]{1,0:T(8,128)(2,1)} %reshape.147, bf16[]{:T(256)} %constant.11.clone.1), kind=kCustom, calls=%fused_computation.2 | custom fusion | bytes 4194816 | tf_op jit(solution)/shard_map/scatter | solution.py:33
  65.2 1.2 constant_dynamic-slice_fusion
  66.4 0.2 copy.92
  66.5 0.2 copy.93
  66.7 14.5 %all_to_all.28 = bf16[16,8,1024]{2,1,0:T(8,128)(2,1)S(1)} all-to-all(bf16[16,8,1024]{2,1,0:T(8,128)(2,1)S(1)} %copy.93), channel_id=1, replica_groups=mesh['ep'=16,'tp'=16] {'ep'}, dimensions={0} | all-to-all | bytes 524288 | tf_op jit(solution)/shard_map/all_to_all | solution.py:61
  81.2 0.1 copy.94
  81.4 0.2 copy.95
  81.7 11.3 %all-gather.6.cloned.1.call-done = bf16[1572864]{0:T(1024)(128)(2,1)} async-done(((bf16[98304]{0:T(1024)(128)(2,1)}), bf16[1572864]{0:T(1024)(128)(2,1)}) %all-gather.6.cloned.1.call-update) | async-done | bytes 3145744 | tf_op jit(solution)/shard_map/all_gather | solution.py:17
  93.0 2.8 %reshape.151 = bf16[16,98304]{1,0:T(8,128)(2,1)S(1)} reshape(bf16[1572864]{0:T(1024)(128)(2,1)} %all-gather.6.cloned.1.call-done) | data formatting | bytes 6291456 | tf_op jit(solution)/shard_map/all_gather | solution.py:17
  95.7 1.8 fusion.17
  97.6 9.6 %reshape.126 = bf16[16,2,1024,16]{3,2,1,0:T(8,128)(2,1)} reshape(bf16[16,32768]{1,0:T(8,128)(2,1)} %get-tuple-element.7) | data formatting | bytes 2097152 | tf_op jit(solution)/shard_map/reshape | solution.py:19
  107.2 6.8 %copy.98 = bf16[2,1024,16,16]{1,3,2,0:T(8,128)(2,1)S(1)} copy(bf16[2,1024,16,16]{3,1,0,2:T(8,128)(2,1)} %bitcast.51) | data formatting | bytes 2097152 | tf_op jit(solution)/shard_map/transpose | solution.py:12
  114.0 8.9 %reshape.128 = bf16[16,2,1024,16]{3,2,1,0:T(8,128)(2,1)} reshape(bf16[16,32768]{1,0:T(8,128)(2,1)S(1)} %copy-done) | data formatting | bytes 2097152 | tf_op jit(solution)/shard_map/reshape | solution.py:19
  122.9 6.8 %copy.100 = bf16[2,1024,16,16]{1,3,2,0:T(8,128)(2,1)S(1)} copy(bf16[2,1024,16,16]{3,1,0,2:T(8,128)(2,1)} %bitcast.52) | data formatting | bytes 2097152 | tf_op jit(solution)/shard_map/transpose | solution.py:12
  129.7 0.6 copy.116
  130.4 0.4 fusion.18
  130.8 0.7 convolution_convert_fusion
  131.7 1.4 copy.103
  133.1 2.1 %reshape.157 = bf16[16,2,4096]{2,1,0:T(2,128)(2,1)S(1)} reshape(bf16[1024,2,4,16]{3,2,1,0:T(4,128)(2,1)S(1)} %bitcast.55) | data formatting | bytes 524288
  135.3 16.0 %all_to_all.29 = bf16[16,2,4096]{2,1,0:T(2,128)(2,1)S(1)} all-to-all(bf16[16,2,4096]{2,1,0:T(2,128)(2,1)S(1)} %reshape.157), channel_id=1, replica_groups=mesh['ep'=16,'tp'=16] {'tp'}, dimensions={0} | all-to-all | bytes 524288 | tf_op jit(solution)/shard_map/all_to_all | solution.py:72
  151.3 1.4 reshape.158
  152.7 1.6 copy.113
  154.3 1.1 copy.106
  155.4 6.5 %all-to-all-start.2 = ((bf16[16,128,64]{1,2,0:T(8,128)(2,1)}), bf16[16,128,64]{1,2,0:T(8,128)(2,1)S(1)}, u32[]{:S(2)}, u32[]{:S(2)}) async-start(bf16[16,128,64]{1,2,0:T(8,128)(2,1)} %copy.106), calls=%async_computation.2 | async-start | bytes 524288 | tf_op jit(solution)/shard_map/all_to_all | solution.py:74
  162.1 0.2 reshape.137
  162.5 8.0 %all-to-all-done.2 = bf16[16,128,64]{1,2,0:T(8,128)(2,1)S(1)} async-done(((bf16[16,128,64]{1,2,0:T(8,128)(2,1)}), bf16[16,128,64]{1,2,0:T(8,128)(2,1)S(1)}, u32[]{:S(2)}, u32[]{:S(2)}) %all-to-all-start.2) | async-done | bytes 262176 | tf_op jit(solution)/shard_map/all_to_all | solution.py:74
  170.5 0.3 copy.107
  170.8 3.2 %gather_fusion = bf16[1024,64]{1,0:T(8,128)(2,1)S(1)} fusion(bf16[2048,64]{1,0:T(8,128)(2,1)S(1)} %bitcast.53, s32[1024]{0:T(1024)S(1)} %broadcast_clamp_fusion), kind=kCustom, calls=%fused_computation | custom fusion | bytes 266240 | tf_op jit(solution)/shard_map/gather | solution.py:77
  174.1 2.8 %fusion.3 = bf16[512,64]{1,0:T(8,128)(2,1)S(1)} fusion(bf16[512,2,64]{2,1,0:T(2,128)(2,1)S(1)} %bitcast.63, f32[512,2]{1,0:T(8,128)S(1)} %copy.85), kind=kLoop, calls=%fused_computation.8 | loop fusion | flops 163840 | bytes 200704 | tf_op jit(solution)/shard_map/reduce_sum | solution.py:78
  176.9 0.7 copy.109
  (30 shorter events, 1.3 us)
Async XLA Ops:
  6.5 7.1 %copy-start.2 = (s32[512,2]{0,1:T(2,128)S(1)}, s32[512,2]{0,1:T(2,128)}, u32[]{:S(2)}) copy-start(s32[512,2]{0,1:T(2,128)} %param.9) | copy-start | bytes 12292
  6.5 45.5 %all-gather.4.cloned.1.call-start = ((), (), s32[]{:S(2)}) async-start(), calls=%async_computation.3 | async-start | bytes 1114112 | tf_op jit(solution)/shard_map/all_gather | solution.py:56
  9.1 83.9 %all-gather.6.cloned.1.call-start = ((), (), s32[]{:S(2)}) async-start(), calls=%async_computation.4 | async-start | bytes 3342336 | tf_op jit(solution)/shard_map/all_gather | solution.py:17
  107.2 6.8 %copy-start = (bf16[16,32768]{1,0:T(8,128)(2,1)S(1)}, bf16[16,32768]{1,0:T(8,128)(2,1)}, u32[]{:S(2)}) copy-start(bf16[16,32768]{1,0:T(8,128)(2,1)} %get-tuple-element.9) | copy-start | bytes 3145732
  122.9 6.8 %copy-start.1 = (bf16[16,32768]{1,0:T(8,128)(2,1)S(1)}, bf16[16,32768]{1,0:T(8,128)(2,1)}, u32[]{:S(2)}) copy-start(bf16[16,32768]{1,0:T(8,128)(2,1)} %get-tuple-element.8) | copy-start | bytes 3145732
  151.3 11.0 %copy-start.3 = (f32[512,2]{0,1:T(2,128)S(1)}, f32[512,2]{0,1:T(2,128)}, u32[]{:S(2)}) copy-start(f32[512,2]{0,1:T(2,128)} %param.10) | copy-start | bytes 12292
  155.4 15.1 %all-to-all-start.2 = ((bf16[16,128,64]{1,2,0:T(8,128)(2,1)}), bf16[16,128,64]{1,2,0:T(8,128)(2,1)S(1)}, u32[]{:S(2)}, u32[]{:S(2)}) async-start(bf16[16,128,64]{1,2,0:T(8,128)(2,1)} %copy.106), calls=%async_computation.2 | async-start | bytes 524288 | tf_op jit(solution)/shard_map/all_to_all | solution.py:74
Sparse Core Ops, SparseCore 0:
  9.2 42.7 all-gather.3
  53.8 39.0 all-gather.5
where the time goes:
time: 185 us; the launch traced here: 184 us
  local copies, waits for them, and re-layouts  70.2 us (38%)
  waiting for transfers between devices  47 us (25%)
  blocking collectives  30.5 us (16%)
  other arithmetic  15.3 us (8%)
  between operations  13.7 us (7%)
  starting transfers between devices  6.57 us (4%)
    all_gather x1, waiting for transfers between devices, body(): group = lax.all_gather(normed, 'tp', axis=0, tiled=True)  27.6 us
    reshape x2, local copies, waits for them, and re-layouts, gather_together(): parts = lines[:, at:at + a.size].reshape(-1, *a.shape)  18.6 us
    all_to_all x1, blocking collectives, body(): lax.all_to_all(produced, 'tp', split_axis=3, concat_axis=2, tiled=True)  16 us
    all_to_all x1, blocking collectives, body(): landed = lax.all_to_all(mine, 'ep', split_axis=0, concat_axis=0, tiled=True)  14.5 us
    transpose x3, local copies, waits for them, and re-layouts, in_order(): return jnp.moveaxis(parts, 0, dim).reshape(shape)  13.7 us
    all_gather x1, waiting for transfers between devices, gather_together(): lines, at, outs = (lax.all_gather(flat, axis), 0, [])  11.3 us
    another operation x2, other arithmetic  9.04 us
    scatter x1, local copies, waits for them, and re-layouts, fill_buffer(): return buffer.at[flat_target].set(jnp.repeat(group, 2, axis=0))  8.55 us
  transfers between devices with their start and end apart: 3, of which 3 were waited for; matrix products, arithmetic and copies ran while one was open for 17% of the time, Pallas kernels for 0%

commit v1 on v0

--- a/solution.py
+++ b/solution.py
@@ -69,7 +69,19 @@
         "erh,ehd->erd", hidden, full_down, preferred_element_type=jnp.float32
     ).astype(jnp.bfloat16)
     produced = produced.reshape(local_experts, ep_size, slice_len, model_width)
-    blocks = lax.all_to_all(produced, "tp", split_axis=3, concat_axis=2, tiled=True)
+    ways, here = (lax.axis_size("tp"), lax.axis_index("tp"))
+    width = produced.shape[3] // ways
+    shape_2 = list(produced.shape)
+    shape_2[3] = width
+    height = shape_2[2]
+    shape_2[2] = height * ways
+    full = jnp.zeros(shape_2, produced.dtype)
+    for mask in range(ways):
+        part = lax.dynamic_slice_in_dim(produced, (here ^ mask) * width, width, axis=3)
+        if mask:
+            part = lax.ppermute(part, "tp", [(d, d ^ mask) for d in range(ways)])
+        full = lax.dynamic_update_slice_in_dim(full, part, (here ^ mask) * height, axis=2)
+    blocks = full
     leaving = blocks.transpose(1, 0, 2, 3).reshape(ep_size, local_experts * capacity, columns)
     returned = lax.all_to_all(leaving, "ep", split_axis=0, concat_axis=0, tiled=True).reshape(
         experts * capacity, columns

time: 185 us -> 2780 us (15.03)
  local copies, waits for them, and re-layouts: 70.2 us -> 2650 us
  starting transfers between devices: 6.57 us -> 39.5 us
  blocking collectives: 30.5 us -> 0 us
    dynamic_update_slice x0 -> x16, local copies, waits for them, and re-layouts: none -> 2570 us  [body(): lax.dynamic_update_slice_in_dim(full, part, (here ^ mask) * height, axis=2)]
    all_to_all x2 -> x0, blocking collectives: 30.5 us -> none  [the longest x1 16 us: body(): lax.all_to_all(produced, 'tp', split_axis=3, concat_axis=2, tiled=True)]
  transfers between devices with their start and end apart: 3 -> 19, of which waited for: 3 -> 4; matrix products, arithmetic and copies ran while one was open for 17% -> 88% of each run, Pallas kernels for 0% -> 0%
where the time goes in v1:
time: 2780 us; the launch traced here: 2770 us
  local copies, waits for them, and re-layouts  2650 us (95%)
  waiting for transfers between devices  53.4 us (2%)
  starting transfers between devices  39.5 us (1%)
    dynamic_update_slice x16, local copies, waits for them, and re-layouts, body(): lax.dynamic_update_slice_in_dim(full, part, (here ^ mask) * height, axis=2)  2570 us
  transfers between devices with their start and end apart: 19, of which 4 were waited for; matrix products, arithmetic and copies ran while one was open for 88% of the time, Pallas kernels for 0%

profile of v1, /device:TPU:1, one launch (start us, length us, event | category | flops | bytes accessed | tf_op | source)
XLA Modules:
  0.0 2771.7 jit_solution(14235895379025559745)
XLA Ops:
  7.5 1.6 fusion.6
  9.2 1.1 copy.109
  10.6 1.1 copy.110
  14.9 9.0 reduce-window.6
  25.1 26.9 all-gather.4.cloned.1.call-done
  52.0 2.3 broadcast_in_dim.20
  54.3 2.3 reshape.147
  56.6 8.6 scatter_custom_fusion
  65.2 1.2 constant_dynamic-slice_fusion.16
  67.4 6.7 all-to-all-start
  74.2 8.1 all-to-all-done
  82.7 10.3 all-gather.6.cloned.1.call-done
  93.0 2.8 reshape.151
  95.8 1.8 fusion.17
  97.6 9.6 reshape.126
  107.2 6.8 copy.111
  114.0 8.9 reshape.128
  122.9 6.8 copy.113
  134.4 1.3 collective-permute-start.3
  135.7 1.5 collective-permute-start.4
  137.1 2.5 collective-permute-start.5
  139.7 1.1 collective-permute-start.6
  140.8 2.8 collective-permute-start.7
  143.6 2.8 collective-permute-start.8
  147.1 4.1 collective-permute-start.10
  151.5 3.5 collective-permute-start.12
  155.0 1.4 collective-permute-start.13
  156.4 2.1 collective-permute-start.14
  159.3 169.5 %dynamic_update_slice.48 = bf16[2,16,64,64]{2,0,3,1:T(2,128)(2,1)S(1)} dynamic-update-slice(bf16[2,16,64,64]{2,0,3,1:T(2,128)(2,1)S(1)} %broadcast_in_dim.8, bf16[2,16,4,64]{2,0,3,1:T(2,128)(2,1)S(1)} %copy.116, s32[]{:T(128)} %constant.28.clone.1, s32[]{:T(128)} %constant.28.clone.1, s32[]{:T(128)S(6)} %select_n.111, s32[]{:T(128)} %constant.28.clone.1) | dynamic-update-slice | bytes 32772 | tf_op jit(solution)/shard_map/dynamic_update_slice | solution.py:83
  329.3 31.8 %dynamic_update_slice.49 = bf16[2,16,64,64]{2,0,3,1:T(2,128)(2,1)S(1)} dynamic-update-slice(bf16[2,16,64,64]{2,0,3,1:T(2,128)(2,1)S(1)} %dynamic_update_slice.48, bf16[2,16,4,64]{2,0,3,1:T(2,128)(2,1)S(1)} %copy.117, s32[]{:T(128)} %constant.28.clone.1, s32[]{:T(128)} %constant.28.clone.1, s32[]{:T(128)S(6)} %select_n.114, s32[]{:T(128)} %constant.28.clone.1) | dynamic-update-slice | bytes 32772 | tf_op jit(solution)/shard_map/dynamic_update_slice | solution.py:83
  361.6 169.5 %dynamic_update_slice.50 = bf16[2,16,64,64]{2,0,3,1:T(2,128)(2,1)S(1)} dynamic-update-slice(bf16[2,16,64,64]{2,0,3,1:T(2,128)(2,1)S(1)} %dynamic_update_slice.49, bf16[2,16,4,64]{2,0,3,1:T(2,128)(2,1)S(1)} %copy.118, s32[]{:T(128)} %constant.28.clone.1, s32[]{:T(128)} %constant.28.clone.1, s32[]{:T(128)S(6)} %select_n.116, s32[]{:T(128)} %constant.28.clone.1) | dynamic-update-slice | bytes 32772 | tf_op jit(solution)/shard_map/dynamic_update_slice | solution.py:83
  531.7 169.5 %dynamic_update_slice.51 = bf16[2,16,64,64]{2,0,3,1:T(2,128)(2,1)S(1)} dynamic-update-slice(bf16[2,16,64,64]{2,0,3,1:T(2,128)(2,1)S(1)} %dynamic_update_slice.50, bf16[2,16,4,64]{2,0,3,1:T(2,128)(2,1)S(1)} %copy.119, s32[]{:T(128)} %constant.28.clone.1, s32[]{:T(128)} %constant.28.clone.1, s32[]{:T(128)S(6)} %select_n.118, s32[]{:T(128)} %constant.28.clone.1) | dynamic-update-slice | bytes 32772 | tf_op jit(solution)/shard_map/dynamic_update_slice | solution.py:83
  701.7 169.5 %dynamic_update_slice.52 = bf16[2,16,64,64]{2,0,3,1:T(2,128)(2,1)S(1)} dynamic-update-slice(bf16[2,16,64,64]{2,0,3,1:T(2,128)(2,1)S(1)} %dynamic_update_slice.51, bf16[2,16,4,64]{2,0,3,1:T(2,128)(2,1)S(1)} %copy.120, s32[]{:T(128)} %constant.28.clone.1, s32[]{:T(128)} %constant.28.clone.1, s32[]{:T(128)S(6)} %select_n.120, s32[]{:T(128)} %constant.28.clone.1) | dynamic-update-slice | bytes 32772 | tf_op jit(solution)/shard_map/dynamic_update_slice | solution.py:83
  871.7 169.5 %dynamic_update_slice.53 = bf16[2,16,64,64]{2,0,3,1:T(2,128)(2,1)S(1)} dynamic-update-slice(bf16[2,16,64,64]{2,0,3,1:T(2,128)(2,1)S(1)} %dynamic_update_slice.52, bf16[2,16,4,64]{2,0,3,1:T(2,128)(2,1)S(1)} %copy.121, s32[]{:T(128)} %constant.28.clone.1, s32[]{:T(128)} %constant.28.clone.1, s32[]{:T(128)S(6)} %select_n.122, s32[]{:T(128)} %constant.28.clone.1) | dynamic-update-slice | bytes 32772 | tf_op jit(solution)/shard_map/dynamic_update_slice | solution.py:83
  1041.7 169.5 %dynamic_update_slice.54 = bf16[2,16,64,64]{2,0,3,1:T(2,128)(2,1)S(1)} dynamic-update-slice(bf16[2,16,64,64]{2,0,3,1:T(2,128)(2,1)S(1)} %dynamic_update_slice.53, bf16[2,16,4,64]{2,0,3,1:T(2,128)(2,1)S(1)} %copy.122, s32[]{:T(128)} %constant.28.clone.1, s32[]{:T(128)} %constant.28.clone.1, s32[]{:T(128)S(6)} %select_n.124, s32[]{:T(128)} %constant.28.clone.1) | dynamic-update-slice | bytes 32772 | tf_op jit(solution)/shard_map/dynamic_update_slice | solution.py:83
  1211.7 169.5 %dynamic_update_slice.55 = bf16[2,16,64,64]{2,0,3,1:T(2,128)(2,1)S(1)} dynamic-update-slice(bf16[2,16,64,64]{2,0,3,1:T(2,128)(2,1)S(1)} %dynamic_update_slice.54, bf16[2,16,4,64]{2,0,3,1:T(2,128)(2,1)S(1)} %copy.123, s32[]{:T(128)} %constant.28.clone.1, s32[]{:T(128)} %constant.28.clone.1, s32[]{:T(128)S(6)} %select_n.126, s32[]{:T(128)} %constant.28.clone.1) | dynamic-update-slice | bytes 32772 | tf_op jit(solution)/shard_map/dynamic_update_slice | solution.py:83
  1381.8 169.7 %dynamic_update_slice.56 = bf16[2,16,64,64]{2,0,3,1:T(2,128)(2,1)S(1)} dynamic-update-slice(bf16[2,16,64,64]{2,0,3,1:T(2,128)(2,1)S(1)} %dynamic_update_slice.55, bf16[2,16,4,64]{2,0,3,1:T(2,128)(2,1)S(1)} %copy.124, s32[]{:T(128)} %constant.28.clone.1, s32[]{:T(128)} %constant.28.clone.1, s32[]{:T(128)S(6)} %select_n.128, s32[]{:T(128)} %constant.28.clone.1) | dynamic-update-slice | bytes 32772 | tf_op jit(solution)/shard_map/dynamic_update_slice | solution.py:83
  1551.9 169.5 %dynamic_update_slice.57 = bf16[2,16,64,64]{2,0,3,1:T(2,128)(2,1)S(1)} dynamic-update-slice(bf16[2,16,64,64]{2,0,3,1:T(2,128)(2,1)S(1)} %dynamic_update_slice.56, bf16[2,16,4,64]{2,0,3,1:T(2,128)(2,1)S(1)} %copy.125, s32[]{:T(128)} %constant.28.clone.1, s32[]{:T(128)} %constant.28.clone.1, s32[]{:T(128)S(6)} %select_n.130, s32[]{:T(128)} %constant.28.clone.1) | dynamic-update-slice | bytes 32772 | tf_op jit(solution)/shard_map/dynamic_update_slice | solution.py:83
  1722.0 169.5 %dynamic_update_slice.58 = bf16[2,16,64,64]{2,0,3,1:T(2,128)(2,1)S(1)} dynamic-update-slice(bf16[2,16,64,64]{2,0,3,1:T(2,128)(2,1)S(1)} %dynamic_update_slice.57, bf16[2,16,4,64]{2,0,3,1:T(2,128)(2,1)S(1)} %copy.126, s32[]{:T(128)} %constant.28.clone.1, s32[]{:T(128)} %constant.28.clone.1, s32[]{:T(128)S(6)} %select_n.132, s32[]{:T(128)} %constant.28.clone.1) | dynamic-update-slice | bytes 32772 | tf_op jit(solution)/shard_map/dynamic_update_slice | solution.py:83
  1892.0 169.5 %dynamic_update_slice.59 = bf16[2,16,64,64]{2,0,3,1:T(2,128)(2,1)S(1)} dynamic-update-slice(bf16[2,16,64,64]{2,0,3,1:T(2,128)(2,1)S(1)} %dynamic_update_slice.58, bf16[2,16,4,64]{2,0,3,1:T(2,128)(2,1)S(1)} %copy.127, s32[]{:T(128)} %constant.28.clone.1, s32[]{:T(128)} %constant.28.clone.1, s32[]{:T(128)S(6)} %select_n.134, s32[]{:T(128)} %constant.28.clone.1) | dynamic-update-slice | bytes 32772 | tf_op jit(solution)/shard_map/dynamic_update_slice | solution.py:83
  2062.0 169.5 %dynamic_update_slice.60 = bf16[2,16,64,64]{2,0,3,1:T(2,128)(2,1)S(1)} dynamic-update-slice(bf16[2,16,64,64]{2,0,3,1:T(2,128)(2,1)S(1)} %dynamic_update_slice.59, bf16[2,16,4,64]{2,0,3,1:T(2,128)(2,1)S(1)} %copy.128, s32[]{:T(128)} %constant.28.clone.1, s32[]{:T(128)} %constant.28.clone.1, s32[]{:T(128)S(6)} %select_n.136, s32[]{:T(128)} %constant.28.clone.1) | dynamic-update-slice | bytes 32772 | tf_op jit(solution)/shard_map/dynamic_update_slice | solution.py:83
  2232.1 169.5 %dynamic_update_slice.61 = bf16[2,16,64,64]{2,0,3,1:T(2,128)(2,1)S(1)} dynamic-update-slice(bf16[2,16,64,64]{2,0,3,1:T(2,128)(2,1)S(1)} %dynamic_update_slice.60, bf16[2,16,4,64]{2,0,3,1:T(2,128)(2,1)S(1)} %copy.129, s32[]{:T(128)} %constant.28.clone.1, s32[]{:T(128)} %constant.28.clone.1, s32[]{:T(128)S(6)} %select_n.138, s32[]{:T(128)} %constant.28.clone.1) | dynamic-update-slice | bytes 32772 | tf_op jit(solution)/shard_map/dynamic_update_slice | solution.py:83
  2402.1 169.5 %dynamic_update_slice.62 = bf16[2,16,64,64]{2,0,3,1:T(2,128)(2,1)S(1)} dynamic-update-slice(bf16[2,16,64,64]{2,0,3,1:T(2,128)(2,1)S(1)} %dynamic_update_slice.61, bf16[2,16,4,64]{2,0,3,1:T(2,128)(2,1)S(1)} %copy.130, s32[]{:T(128)} %constant.28.clone.1, s32[]{:T(128)} %constant.28.clone.1, s32[]{:T(128)S(6)} %select_n.140, s32[]{:T(128)} %constant.28.clone.1) | dynamic-update-slice | bytes 32772 | tf_op jit(solution)/shard_map/dynamic_update_slice | solution.py:83
  2572.1 169.5 %dynamic_update_slice.63 = bf16[2,16,64,64]{2,0,3,1:T(2,128)(2,1)S(1)} dynamic-update-slice(bf16[2,16,64,64]{2,0,3,1:T(2,128)(2,1)S(1)} %dynamic_update_slice.62, bf16[2,16,4,64]{2,0,3,1:T(2,128)(2,1)S(1)} %copy.131, s32[]{:T(128)} %constant.28.clone.1, s32[]{:T(128)} %constant.28.clone.1, s32[]{:T(128)S(6)} %select_n.142, s32[]{:T(128)} %constant.28.clone.1) | dynamic-update-slice | bytes 32772 | tf_op jit(solution)/shard_map/dynamic_update_slice | solution.py:83
  2742.6 6.5 all-to-all-start.1
  2749.6 8.0 all-to-all-done.1
  2757.9 3.2 gather_fusion
  2761.1 2.8 fusion.3
  (90 shorter events, 23.4 us)
Async XLA Ops:
  6.5 18.2 copy-start.2
  6.5 45.5 %all-gather.4.cloned.1.call-start = ((), (), s32[]{:S(2)}) async-start(), calls=%async_computation.2 | async-start | bytes 1114112 | tf_op jit(solution)/shard_map/all_gather | solution.py:56
  9.1 83.9 %all-gather.6.cloned.1.call-start = ((), (), s32[]{:S(2)}) async-start(), calls=%async_computation.3 | async-start | bytes 3342336 | tf_op jit(solution)/shard_map/all_gather | solution.py:17
  67.4 14.9 all-to-all-start
  107.2 6.8 copy-start
  122.9 6.8 copy-start.1
  132.2 5.0 collective-permute-start
  132.6 7.1 collective-permute-start.1
  133.4 7.4 collective-permute-start.2
  134.4 9.2 collective-permute-start.3
  135.7 10.7 collective-permute-start.4
  137.1 10.0 collective-permute-start.5
  139.7 11.5 collective-permute-start.6
  140.8 10.7 collective-permute-start.7
  143.6 11.4 collective-permute-start.8
  146.3 10.0 collective-permute-start.9
  147.1 1744.4 %collective-permute-start.10 = (bf16[2,16,4,64]{3,2,1,0:T(4,128)(2,1)S(1)}, bf16[2,16,4,64]{3,2,1,0:T(4,128)(2,1)S(1)}, u32[]{:S(2)}, u32[]{:S(2)}) collective-permute-start(bf16[2,16,4,64]{3,2,1,0:T(4,128)(2,1)S(1)} %get-tuple-element.14), channel_id=1, source_target_pairs={{0,11},{1,10},{2,9},{3,8},{4,15},{5,14},{6,13},{7,12},{8,3},{9,2},... | collective-permute-start | bytes 49160 | tf_op jit(solution)/shard_map/ppermute | solution.py:82
  151.2 1910.3 %collective-permute-start.11 = (bf16[2,16,4,64]{3,2,1,0:T(4,128)(2,1)S(1)}, bf16[2,16,4,64]{3,2,1,0:T(4,128)(2,1)S(1)}, u32[]{:S(2)}, u32[]{:S(2)}) collective-permute-start(bf16[2,16,4,64]{3,2,1,0:T(4,128)(2,1)S(1)} %get-tuple-element.13), channel_id=1, source_target_pairs={{0,12},{1,13},{2,14},{3,15},{4,8},{5,9},{6,10},{7,11},{8,4},{9,5},... | collective-permute-start | bytes 49160 | tf_op jit(solution)/shard_map/ppermute | solution.py:82
  151.5 2080.1 %collective-permute-start.12 = (bf16[2,16,4,64]{3,2,1,0:T(4,128)(2,1)S(1)}, bf16[2,16,4,64]{3,2,1,0:T(4,128)(2,1)S(1)}, u32[]{:S(2)}, u32[]{:S(2)}) collective-permute-start(bf16[2,16,4,64]{3,2,1,0:T(4,128)(2,1)S(1)} %get-tuple-element.12), channel_id=1, source_target_pairs={{0,13},{1,12},{2,15},{3,14},{4,9},{5,8},{6,11},{7,10},{8,5},{9,4},... | collective-permute-start | bytes 49160 | tf_op jit(solution)/shard_map/ppermute | solution.py:82
  155.0 2246.6 %collective-permute-start.13 = (bf16[2,16,4,64]{3,2,1,0:T(4,128)(2,1)S(1)}, bf16[2,16,4,64]{3,2,1,0:T(4,128)(2,1)S(1)}, u32[]{:S(2)}, u32[]{:S(2)}) collective-permute-start(bf16[2,16,4,64]{3,2,1,0:T(4,128)(2,1)S(1)} %get-tuple-element.11), channel_id=1, source_target_pairs={{0,14},{1,15},{2,12},{3,13},{4,10},{5,11},{6,8},{7,9},{8,6},{9,7},... | collective-permute-start | bytes 49160 | tf_op jit(solution)/shard_map/ppermute | solution.py:82
  156.4 2415.2 %collective-permute-start.14 = (bf16[2,16,4,64]{3,2,1,0:T(4,128)(2,1)S(1)}, bf16[2,16,4,64]{3,2,1,0:T(4,128)(2,1)S(1)}, u32[]{:S(2)}, u32[]{:S(2)}) collective-permute-start(bf16[2,16,4,64]{3,2,1,0:T(4,128)(2,1)S(1)} %get-tuple-element.10), channel_id=1, source_target_pairs={{0,15},{1,14},{2,13},{3,12},{4,11},{5,10},{6,9},{7,8},{8,7},{9,6},... | collective-permute-start | bytes 49160 | tf_op jit(solution)/shard_map/ppermute | solution.py:82
  2061.5 687.9 %copy-start.3 = (f32[512,2]{0,1:T(2,128)S(1)}, f32[512,2]{0,1:T(2,128)}, u32[]{:S(2)}) copy-start(f32[512,2]{0,1:T(2,128)} %param.10) | copy-start | bytes 12292
  2742.6 15.0 all-to-all-start.1
Sparse Core Ops, SparseCore 0:
  9.2 42.7 all-gather.3
  53.8 39.1 all-gather.5
